TPU v7x, 32 devices: a whole 2x2x4 slice. The times are simulated.
32 devices in a mesh: fs: 8 (over z, x), tp: 4 (over y, core).
Axes of the slice: x: 2, y: 2, z: 4, core: 2. Of those that a mesh axis runs over, the one named last changes fastest.
Arguments:
- tokens: bfloat16 [64, 2048], P(('fs', 'tp')), may hold values from -6 to 6
- route_experts: int32 [64, 2], P(('fs', 'tp')), may hold values from 0 to 3, as said below
- route_logits: float32 [64, 2], P(('fs', 'tp')), may hold values from -8 to 8
- norm_gain: float32 [2048], P('fs'), may hold values from 0.1 to 1.9
- gate_train: float32 [4, 2048, 8192], P(None, 'fs', 'tp'), may hold values from -0.125 to 0.125
- up_train: float32 [4, 2048, 8192], P(None, 'fs', 'tp'), may hold values from -0.125 to 0.125
- down_train: float32 [4, 2048, 8192], P(None, 'fs', 'tp'), may hold values from -0.125 to 0.125
Outputs:
- gate_serve: bfloat16 [8, 2048, 4096], P('fs')
- up_serve: bfloat16 [8, 2048, 4096], P('fs')
- down_serve: bfloat16 [8, 2048, 4096], P('fs')
- mixed: bfloat16 [64, 2048], P(('fs', 'tp'))
Inputs may be any that keep to these rules, and one draw needn't show every extreme that they name: `route_experts`: the two experts of a row differ; any expert may be named by every row of the devices that share one index along tp, and in every draw some expert is.
All inputs are finite; a program needn't handle non-finite values.
Results may differ from a plain program's by a relative error of at most 0.0085.
Values may be sent and summed in bfloat16 or wider, within the bound.
A program may use at most 192 MiB of HBM per device.

v0:
```python
import jax
import jax.numpy as jnp
from jax import lax
from jax.sharding import PartitionSpec as P


def for_sending(array):
    return jax.tree.map(lambda a: a.astype(jnp.bfloat16) if a.dtype == jnp.float32 else a, array)


def normalize(tokens):
    values = tokens.astype(jnp.float32)
    row_mean = jnp.mean(values, axis=-1, keepdims=True)
    centered = values - row_mean
    row_var = jnp.mean(centered * centered, axis=-1, keepdims=True)
    return (centered * lax.rsqrt(row_var + 1e-05)).astype(jnp.bfloat16)


def per_device(tokens, route_experts, route_logits, norm_gain, gate_train, up_train, down_train):
    fs_size = lax.axis_size("fs")
    tp_size = lax.axis_size("tp")
    expert_count = gate_train.shape[0]
    slices = fs_size // expert_count
    scale = norm_gain[None, :, None]
    gate_half = (scale * gate_train).astype(jnp.bfloat16)
    up_half = (scale * up_train).astype(jnp.bfloat16)
    down_half = down_train.astype(jnp.bfloat16)
    swapped = (
        lax.all_to_all(gate_half, "tp", split_axis=1, concat_axis=2, tiled=True),
        lax.all_to_all(up_half, "tp", split_axis=1, concat_axis=2, tiled=True),
        lax.all_to_all(down_half, "tp", split_axis=1, concat_axis=2, tiled=True),
    )
    quarter = swapped[0].shape[1]
    hidden_total = swapped[0].shape[2]
    block_width = hidden_total // slices

    def split_quarter(matrix):
        blocks = matrix.reshape(expert_count, quarter, slices, block_width)
        return blocks.transpose(0, 2, 1, 3).reshape(expert_count * slices, quarter, block_width)

    owned = lax.all_to_all(
        for_sending(tuple((split_quarter(matrix) for matrix in swapped))),
        "fs",
        split_axis=0,
        concat_axis=1,
        tiled=True,
    )
    stacked = tuple((matrix.reshape(1, fs_size, 1, quarter, block_width) for matrix in owned))
    joined = jax.tree.map(
        lambda part, own: part.astype(own.dtype),
        lax.all_gather(for_sending(stacked), "tp", axis=2, tiled=True),
        stacked,
    )
    gate_serve, up_serve, down_serve = tuple(
        (matrix.reshape(1, fs_size * tp_size * quarter, block_width) for matrix in joined)
    )
    normed = normalize(tokens)
    first = jax.nn.sigmoid(route_logits[:, 0] - route_logits[:, 1])
    second = jax.nn.sigmoid(route_logits[:, 1] - route_logits[:, 0])
    labels = jnp.arange(expert_count, dtype=jnp.int32)
    table = first[:, None] * (route_experts[:, 0:1] == labels[None, :]).astype(jnp.float32)
    table = table + second[:, None] * (route_experts[:, 1:2] == labels[None, :]).astype(jnp.float32)
    table = table.astype(jnp.bfloat16)
    rows_all, table_all = (
        lax.all_gather(normed, "fs", axis=0, tiled=True),
        lax.all_gather(table, "fs", axis=0, tiled=True),
    )
    own_expert = lax.axis_index("fs") // slices
    selector = (labels == own_expert).astype(jnp.float32)
    weight = jnp.sum(table_all.astype(jnp.float32) * selector[None, :], axis=1)
    gate_act = jnp.dot(rows_all, gate_serve[0], preferred_element_type=jnp.float32)
    up_act = jnp.dot(rows_all, up_serve[0], preferred_element_type=jnp.float32)
    hidden = (weight[:, None] * jax.nn.silu(gate_act) * up_act).astype(jnp.bfloat16)
    down_own = down_serve[0]
    summed = lax.psum_scatter(
        lax.dot_general(
            hidden, down_own, (((1,), (1,)), ((), ())), preferred_element_type=jnp.float32
        ),
        "fs",
        scatter_dimension=0,
        tiled=True,
    )
    return (gate_serve, up_serve, down_serve, summed.astype(jnp.bfloat16))


def solution(mesh):
    return jax.shard_map(
        per_device,
        mesh=mesh,
        in_specs=(
            P(("fs", "tp"), None),
            P(("fs", "tp"), None),
            P(("fs", "tp"), None),
            P("fs"),
            P(None, "fs", "tp"),
            P(None, "fs", "tp"),
            P(None, "fs", "tp"),
        ),
        out_specs=(
            P("fs", None, None),
            P("fs", None, None),
            P("fs", None, None),
            P(("fs", "tp"), None),
        ),
        check_vma=False,
    )
```

profile of v0, /device:TPU:0, one launch (start us, length us, event | category | flops | bytes accessed | tf_op | source)
XLA Modules:
  0.0 835.1 jit_solution(11731693331885910002)
XLA Ops:
  7.2 11.9 %multiply_convert_fusion = (bf16[4,256,2048]{2,1,0:T(8,128)(2,1)}, bf16[4,256,2048]{2,1,0:T(8,128)(2,1)}) fusion(f32[4,256,2048]{2,1,0:T(8,128)} %param.12, f32[256]{0:T(256)} %param.10, f32[4,256,2048]{2,1,0:T(8,128)} %param.11), kind=kLoop, calls=%fused_computation.1 | loop fusion | flops 8388608 | bytes 25166848 | tf_op jit(solution)/shard_map/convert_element_type | solution.py:26
  19.1 5.4 copy.29
  24.5 52.5 %all_to_all.72 = bf16[4,256,2048]{2,0,1:T(4,128)(2,1)S(1)} all-to-all(bf16[4,256,2048]{2,0,1:T(4,128)(2,1)S(1)} %copy.29), channel_id=1, replica_groups=mesh['fs'=8,'tp'=4] {'tp'}, dimensions={1} | all-to-all | bytes 8388608 | tf_op jit(solution)/shard_map/all_to_all | solution.py:29
  77.0 5.2 copy.45
  82.3 10.2 %reshape.78 = bf16[4,64,2,4096]{3,2,1,0:T(2,128)(2,1)} reshape(bf16[4,64,4,2048]{3,2,1,0:T(4,128)(2,1)} %bitcast.45) | data formatting | bytes 8388608 | tf_op jit(solution)/shard_map/reshape | solution.py:38
  97.6 98.7 %all_to_all.73 = bf16[8,64,4096]{2,1,0:T(8,128)(2,1)} all-to-all(bf16[8,64,4096]{2,1,0:T(8,128)(2,1)S(1)} %bitcast.47), channel_id=1, replica_groups=mesh['fs'=8,'tp'=4] {'fs'}, dimensions={0} | all-to-all | bytes 8388608 | tf_op jit(solution)/shard_map/all_to_all | solution.py:41
  196.9 8.8 %copy.42 = bf16[4,256,2048]{2,0,1:T(4,128)(2,1)S(1)} copy(f32[4,256,2048]{2,1,0:T(8,128)} %param.13) | data formatting | bytes 12582912 | tf_op args[6]
  205.7 96.2 %all_to_all.74 = bf16[4,256,2048]{2,0,1:T(4,128)(2,1)S(1)} all-to-all(bf16[4,256,2048]{2,0,1:T(4,128)(2,1)S(1)} %copy.42), channel_id=1, replica_groups=mesh['fs'=8,'tp'=4] {'tp'}, dimensions={1} | all-to-all | bytes 8388608 | tf_op jit(solution)/shard_map/all_to_all | solution.py:31
  301.9 5.2 copy.43
  307.2 10.2 %reshape.86 = bf16[4,64,2,4096]{3,2,1,0:T(2,128)(2,1)} reshape(bf16[4,64,4,2048]{3,2,1,0:T(4,128)(2,1)} %bitcast.49) | data formatting | bytes 8388608 | tf_op jit(solution)/shard_map/reshape | solution.py:38
  322.5 96.6 %all_to_all.75 = bf16[8,64,4096]{2,1,0:T(8,128)(2,1)} all-to-all(bf16[8,64,4096]{2,1,0:T(8,128)(2,1)S(1)} %bitcast.51), channel_id=1, replica_groups=mesh['fs'=8,'tp'=4] {'fs'}, dimensions={0} | all-to-all | bytes 8388608 | tf_op jit(solution)/shard_map/all_to_all | solution.py:41
  419.2 5.4 copy.32
  424.7 95.7 %all_to_all.76 = bf16[4,256,2048]{2,0,1:T(4,128)(2,1)S(1)} all-to-all(bf16[4,256,2048]{2,0,1:T(4,128)(2,1)S(1)} %copy.32), channel_id=1, replica_groups=mesh['fs'=8,'tp'=4] {'tp'}, dimensions={1} | all-to-all | bytes 8388608 | tf_op jit(solution)/shard_map/all_to_all | solution.py:30
  525.6 10.2 %reshape.82 = bf16[4,64,2,4096]{3,2,1,0:T(2,128)(2,1)} reshape(bf16[4,64,4,2048]{3,2,1,0:T(4,128)(2,1)} %bitcast.53) | data formatting | bytes 8388608 | tf_op jit(solution)/shard_map/reshape | solution.py:38
  541.0 96.4 %all_to_all.77 = bf16[8,64,4096]{2,1,0:T(8,128)(2,1)} all-to-all(bf16[8,64,4096]{2,1,0:T(8,128)(2,1)S(1)} %bitcast.55), channel_id=1, replica_groups=mesh['fs'=8,'tp'=4] {'fs'}, dimensions={0} | all-to-all | bytes 8388608 | tf_op jit(solution)/shard_map/all_to_all | solution.py:41
  637.9 30.5 %all-gather.4 = bf16[8,2,2048]{2,1,0:T(2,128)(2,1)S(1)} all-gather(bf16[1,2,2048]{2,1,0:T(2,128)(2,1)S(1)} %fusion.15), channel_id=1, replica_groups=mesh['fs'=8,'tp'=4] {'fs'}, dimensions={0}, use_global_device_ids=true | all-gather | bytes 73728 | tf_op jit(solution)/shard_map/all_gather | solution.py:65
  670.2 18.6 %all-gather.3 = bf16[8,2,4]{2,1,0:T(2,128)(2,1)S(1)} all-gather(bf16[1,2,4]{2,1,0:T(2,128)(2,1)S(1)} %fusion.20), channel_id=1, replica_groups=mesh['fs'=8,'tp'=4] {'fs'}, dimensions={0}, use_global_device_ids=true | all-gather | bytes 144 | tf_op jit(solution)/shard_map/all_gather | solution.py:66
  688.9 8.0 fusion.22
  697.0 44.4 %all-gather.11.cloned.1.call-done = bf16[8,256,4096]{2,1,0:T(8,128)(2,1)} async-done(((bf16[8,64,4096]{2,1,0:T(8,128)(2,1)}), bf16[8,256,4096]{2,1,0:T(8,128)(2,1)}) %all-gather.11.cloned.1.call-update) | async-done | bytes 16777232 | tf_op jit(solution)/shard_map/all_gather | solution.py:51
  741.3 13.9 %fusion.1 = f32[16,2048]{1,0:T(8,128)S(1)} fusion(bf16[2048,4096]{1,0:T(8,128)(2,1)} %bitcast.38, bf16[16,2048]{1,0:T(8,128)(2,1)S(1)} %reshape.102, bf16[2048,4096]{1,0:T(8,128)(2,1)} %bitcast.42, f32[16,4096]{1,0:T(8,128)S(1)} %fusion.22, f32[16]{0:T(128)S(1)} %fusion.14), kind=kOutput, calls=%fused_computation.8 | convolution fusion | flops 537329664 | bytes 34013248 | tf_op jit(solution)/shard_map/dot_general | solution.py:76
  755.2 38.3 %all-reduce.2 = bf16[16,2048]{1,0:T(8,128)(2,1)S(1)} all-reduce(f32[16,2048]{1,0:T(8,128)S(1)} %fusion.1), channel_id=5, replica_groups=mesh['fs'=8,'tp'=4] {'fs'}, use_global_device_ids=true, to_apply=%region_3.4.clone | all-reduce | flops 32768 | bytes 196608
  794.2 16.8 %copy.51 = bf16[1,2048,4096]{2,1,0:T(8,128)(2,1)} copy(bf16[1,2048,4096]{2,1,0:T(8,128)(2,1)} %bitcast.37) | data formatting | bytes 33554432
  811.0 8.5 %copy.52 = bf16[1,2048,4096]{2,1,0:T(8,128)(2,1)} copy(bf16[1,2048,4096]{2,1,0:T(8,128)(2,1)S(1)} %bitcast.43) | data formatting | bytes 33554432
  822.1 6.2 copy.53
  (44 shorter events, 26.1 us)
Async XLA Ops:
  7.2 681.7 %all-gather.9.cloned.1.call-start = ((), (), s32[]{:S(2)}) async-start(), calls=%async_computation.6 | async-start | bytes 20971520 | tf_op jit(solution)/shard_map/all_gather | solution.py:51
  196.4 500.6 %all-gather.13.cloned.1.call-start = ((), (), s32[]{:S(2)}) async-start(), calls=%async_computation.8 | async-start | bytes 20971520 | tf_op jit(solution)/shard_map/all_gather | solution.py:51
  419.2 322.1 %all-gather.11.cloned.1.call-start = ((), (), s32[]{:S(2)}) async-start(), calls=%async_computation.7 | async-start | bytes 20971520 | tf_op jit(solution)/shard_map/all_gather | solution.py:51
  540.9 96.5 %copy-start.1 = (bf16[2,2048]{1,0:T(2,128)(2,1)S(1)}, bf16[2,2048]{1,0:T(2,128)(2,1)}, u32[]{:S(2)}) copy-start(bf16[2,2048]{1,0:T(2,128)(2,1)} %param.7) | copy-start | bytes 24580
  540.9 127.5 %copy-start.4 = (u32[32]{0:T(128)S(1)}, u32[32]{0:T(128)}, u32[]{:S(2)}) copy-start(u32[32]{0:T(128)} %constant.39) | copy-start | bytes 388
  540.9 128.8 %copy-start.2 = (s32[2,2]{1,0:T(2,128)S(1)}, s32[2,2]{1,0:T(2,128)}, u32[]{:S(2)}) copy-start(s32[2,2]{1,0:T(2,128)} %param.8) | copy-start | bytes 52
  541.0 129.0 %copy-start.3 = (f32[2,2]{1,0:T(2,128)S(1)}, f32[2,2]{1,0:T(2,128)}, u32[]{:S(2)}) copy-start(f32[2,2]{1,0:T(2,128)} %param.9) | copy-start | bytes 52
  794.2 16.8 %copy-start = (bf16[8,256,4096]{2,1,0:T(8,128)(2,1)S(1)}, bf16[8,256,4096]{2,1,0:T(8,128)(2,1)}, u32[]{:S(2)}) copy-start(bf16[8,256,4096]{2,1,0:T(8,128)(2,1)} %all-gather.11.cloned.1.call-done) | copy-start | bytes 50331652
  794.2 25.3 %slice-start = ((s8[16777216]{0:T(1024)(128)(4,1)}), s8[4194304]{0:T(1024)(128)(4,1)S(1)}, s32[]{:S(2)}) async-start(s8[16777216]{0:T(1024)(128)(4,1)} %bitcast.39), calls=%async_computation.9 | async-start | bytes 8388608
  794.2 25.3 %slice-start.1 = ((s8[16777216]{0:T(1024)(128)(4,1)}), s8[4194304]{0:T(1024)(128)(4,1)S(1)}, s32[]{:S(2)}) async-start(s8[16777216]{0:T(1024)(128)(4,1)} %bitcast.39), calls=%async_computation.10 | async-start | bytes 8388608
  811.0 9.9 %slice-start.2 = ((s8[16777216]{0:T(1024)(128)(4,1)}), s8[4194304]{0:T(1024)(128)(4,1)S(1)}, s32[]{:S(2)}) async-start(s8[16777216]{0:T(1024)(128)(4,1)} %bitcast.39), calls=%async_computation.11 | async-start | bytes 8388608
  811.0 11.1 %slice-start.3 = ((s8[16777216]{0:T(1024)(128)(4,1)}), s8[4194304]{0:T(1024)(128)(4,1)S(1)}, s32[]{:S(2)}) async-start(s8[16777216]{0:T(1024)(128)(4,1)} %bitcast.39), calls=%async_computation.12 | async-start | bytes 8388608
Sparse Core Ops, SparseCore 0:
  196.5 148.9 all-gather.8
  419.3 148.2 all-gather.12
  637.5 103.7 all-gather.10
where the time goes:
time: 841 us; the launch traced here: 835 us
  blocking collectives  624 us (74%)
  local copies, waits for them, and re-layouts  117 us (14%)
  waiting for transfers between devices  44.4 us (5%)
  matrix products  21.9 us (3%)
  between operations  14.8 us (2%)
  other arithmetic  12.7 us (2%)
    all_to_all x3, blocking collectives, per_device(): lax.all_to_all(for_sending(tuple((split_quarter(matrix) for matrix in swa...  292 us
    all_to_all x1, blocking collectives, per_device(): lax.all_to_all(down_half, 'tp', split_axis=1, concat_axis=2, tiled=True)  96.2 us
    all_to_all x1, blocking collectives, per_device(): lax.all_to_all(up_half, 'tp', split_axis=1, concat_axis=2, tiled=True)  95.7 us
    all_to_all x1, blocking collectives, per_device(): lax.all_to_all(gate_half, 'tp', split_axis=1, concat_axis=2, tiled=True)  52.5 us
    all_gather x3, waiting for transfers between devices, per_device(): lax.all_gather(for_sending(stacked), 'tp', axis=2, tiled=True)  44.4 us
    unnamed x24, local copies, waits for them, and re-layouts  43.5 us
    unnamed x1, blocking collectives  38.3 us
    reshape x3, local copies, waits for them, and re-layouts, split_quarter(): blocks = matrix.reshape(expert_count, quarter, slices, block_width)  30.7 us
  transfers between devices with their start and end apart: 3, of which 1 were waited for; matrix products, arithmetic and copies ran while one was open for 8% of the time, Pallas kernels for 0%

commit v1 on v0

--- a/solution.py
+++ b/solution.py
@@ -1,7 +1,16 @@
+import functools
+
 import jax
 import jax.numpy as jnp
 from jax import lax
+from jax.experimental import pallas as pl
+from jax.experimental.pallas import tpu as pltpu
 from jax.sharding import PartitionSpec as P
+
+MESH = pl.DeviceIdType.MESH
+PARTS = 2
+LAG_TP = 2
+LAG_FS = 4
 
 
 def for_sending(array):
@@ -16,7 +25,7 @@
     return (centered * lax.rsqrt(row_var + 1e-05)).astype(jnp.bfloat16)
 
 
-def per_device(tokens, route_experts, route_logits, norm_gain, gate_train, up_train, down_train):
+def per_device_general(tokens, route_experts, route_logits, norm_gain, gate_train, up_train, down_train):
     fs_size = lax.axis_size("fs")
     tp_size = lax.axis_size("tp")
     expert_count = gate_train.shape[0]
@@ -83,9 +92,292 @@
     return (gate_serve, up_serve, down_serve, summed.astype(jnp.bfloat16))
 
 
+def round_kernel(gain_ref, gate_ref, up_ref, down_ref, out_ref):
+    gain = gain_ref[...]
+    out_ref[0, 0] = (gain * gate_ref[0]).astype(jnp.bfloat16)
+    out_ref[1, 0] = (gain * up_ref[0]).astype(jnp.bfloat16)
+    out_ref[2, 0] = down_ref[0].astype(jnp.bfloat16)
+
+
+def rounded(norm_gain, gate_train, up_train, down_train):
+    experts, rows, width = gate_train.shape
+    tile = rows // 2
+    weight = pl.BlockSpec((1, tile, width), lambda e, r: (e, r, 0))
+    return pl.pallas_call(
+        round_kernel,
+        grid=(experts, rows // tile),
+        in_specs=[pl.BlockSpec((tile, 1), lambda e, r: (r, 0)), weight, weight, weight],
+        out_specs=pl.BlockSpec((3, 1, tile, width), lambda e, r: (0, e, r, 0)),
+        out_shape=jax.ShapeDtypeStruct((3, experts, rows, width), jnp.bfloat16),
+        name="round_weights",
+    )(norm_gain[:, None], gate_train, up_train, down_train)
+
+
+def exchange_kernel(
+    src, joined, transit, held, l_in, l_out, z_s, z_r, y_s, y_r, x_s, x_r, c_s, c_r
+):
+    matrices, experts, rows, width = src.shape
+    chunk = rows // PARTS
+    pieces = matrices * PARTS * experts
+    f = lax.axis_index("fs")
+    t = lax.axis_index("tp")
+    z, x = lax.div(f, 2), lax.rem(f, 2)
+    s, c = lax.div(t, 2), lax.rem(t, 2)
+    y_peer = (f, (1 - s) * 2 + c)
+    c_peer = (f, s * 2 + 1 - c)
+    x_peer = (z * 2 + 1 - x, t)
+
+    def z_peer(d):
+        return (lax.rem(z + d, experts) * 2 + x, t)
+
+    barrier = pltpu.get_barrier_semaphore()
+    for d in range(1, experts):
+        pl.semaphore_signal(barrier, inc=1, device_id=z_peer(d), device_id_type=MESH)
+    for peer in (y_peer, c_peer, x_peer):
+        pl.semaphore_signal(barrier, inc=1, device_id=peer, device_id_type=MESH)
+
+    def parts_of(k):
+        d = lax.rem(k, experts)
+        g = lax.div(k, experts)
+        return d, g, lax.rem(g, PARTS), lax.div(g, PARTS)
+
+    def final(m, zs, xs, h):
+        row = pl.multiple_of((zs * 2 + xs) * rows + h * chunk, chunk)
+        return joined.at[m, pl.ds(row, chunk), pl.ds(pl.multiple_of(c * width, width), width)]
+
+    def passing(m, zs, h):
+        return transit.at[m, zs, pl.ds(pl.multiple_of(h * chunk, chunk), chunk)]
+
+    def source(m, e, h):
+        return src.at[m, e, pl.ds(pl.multiple_of(h * chunk, chunk), chunk)]
+
+    def remote(a, b, send, recv, peer):
+        return pltpu.make_async_remote_copy(
+            src_ref=a, dst_ref=b, send_sem=send, recv_sem=recv, device_id=peer,
+            device_id_type=MESH,
+        )
+
+    def load(g):
+        return pltpu.make_async_copy(
+            source(lax.div(g, PARTS), z, lax.rem(g, PARTS)), held.at[g], l_in.at[g]
+        )
+
+    @pl.loop(0, matrices * PARTS)
+    def _(g):
+        load(g).start()
+
+    pl.semaphore_wait(barrier, experts + 2)
+
+    def send_z(home):
+        @pl.loop(0, pieces)
+        def _(k):
+            d, g, h, m = parts_of(k)
+
+            @pl.when(d > 0)
+            def _():
+                here = final(m, z, x, h) if home else passing(m, z, h)
+                there = source(m, lax.rem(z + d, experts), h)
+                remote(there, here, z_s.at[k], z_r.at[k], z_peer(d)).start()
+
+            @pl.when(d == 0)
+            def _():
+                here = final(m, z, x, h) if home else passing(m, z, h)
+                load(g).wait()
+                pltpu.make_async_copy(held.at[g], here, l_out.at[g]).start()
+
+    def place(k, keep):
+        d, g, h, m = parts_of(k)
+        zs = lax.rem(z + experts - d, experts)
+        return final(m, zs, x, h) if keep else passing(m, zs, h)
+
+    def forward(k, keep):
+        d, g, h, m = parts_of(k)
+        zs = lax.rem(z + experts - d, experts)
+        if keep:
+            here = final(m, zs, x, h)
+            remote(here, here, c_s.at[k], c_r.at[k], c_peer).start()
+        else:
+            remote(
+                passing(m, zs, h), final(m, zs, x, h), x_s.at[k], x_r.at[k], x_peer
+            ).start()
+
+    def run(home):
+        send_z(home)
+
+        @pl.loop(0, pieces + LAG_FS)
+        def _(i):
+            @pl.when(i < pieces)
+            def _():
+                d, g, h, m = parts_of(i)
+                here = place(i, home)
+
+                @pl.when(d > 0)
+                def _():
+                    remote(here, here, z_s.at[i], z_r.at[i], y_peer).wait_recv()
+
+                @pl.when(d == 0)
+                def _():
+                    pltpu.make_async_copy(held.at[g], here, l_out.at[g]).wait()
+
+                remote(here, here, y_s.at[i], y_r.at[i], y_peer).start()
+                forward(i, home)
+
+            @pl.when((i >= LAG_TP) & (i < pieces + LAG_TP))
+            def _():
+                k = i - LAG_TP
+                here = place(k, not home)
+                remote(here, here, y_s.at[k], y_r.at[k], y_peer).wait_recv()
+                forward(k, not home)
+
+            @pl.when(i >= LAG_FS)
+            def _():
+                k = i - LAG_FS
+                d, g, h, m = parts_of(k)
+                here = final(m, lax.rem(z + experts - d, experts), 1 - x, h)
+                remote(here, here, x_s.at[k], x_r.at[k], x_peer).wait_recv()
+                remote(
+                    here, here, c_s.at[pieces + k], c_r.at[pieces + k], c_peer
+                ).start()
+
+        @pl.loop(0, pieces)
+        def _(k):
+            d, g, h, m = parts_of(k)
+            zs = lax.rem(z + experts - d, experts)
+            here = place(k, home)
+
+            @pl.when(d > 0)
+            def _():
+                remote(
+                    source(m, lax.rem(z + d, experts), h), here, z_s.at[k], z_r.at[k], y_peer
+                ).wait_send()
+
+            remote(here, here, y_s.at[k], y_r.at[k], y_peer).wait_send()
+            remote(passing(m, zs, h), here, x_s.at[k], x_r.at[k], x_peer).wait_send()
+            for q in range(2):
+                xs = x if q == 0 else 1 - x
+                mine = final(m, zs, xs, h)
+                row = pl.multiple_of((zs * 2 + xs) * rows + h * chunk, chunk)
+                other = joined.at[
+                    m, pl.ds(row, chunk), pl.ds(pl.multiple_of((1 - c) * width, width), width)
+                ]
+                n = q * pieces + k
+                remote(mine, other, c_s.at[n], c_r.at[n], c_peer).wait()
+
+    @pl.when(s == x)
+    def _():
+        run(True)
+
+    @pl.when(s != x)
+    def _():
+        run(False)
+
+
+def exchanged(packed, fs_size):
+    matrices, experts, rows, width = packed.shape
+    pieces = matrices * PARTS * experts
+    groups = matrices * PARTS
+    anywhere = pl.BlockSpec(memory_space=pl.ANY)
+    dma = pltpu.SemaphoreType.DMA
+    return pl.pallas_call(
+        exchange_kernel,
+        in_specs=[anywhere],
+        out_specs=[anywhere, anywhere],
+        out_shape=[
+            jax.ShapeDtypeStruct((matrices, fs_size * rows, 2 * width), jnp.bfloat16),
+            jax.ShapeDtypeStruct(packed.shape, jnp.bfloat16),
+        ],
+        scratch_shapes=[
+            pltpu.VMEM((groups, rows // PARTS, width), jnp.bfloat16),
+            dma((groups,)),
+            dma((groups,)),
+            dma((pieces,)),
+            dma((pieces,)),
+            dma((pieces,)),
+            dma((pieces,)),
+            dma((pieces,)),
+            dma((pieces,)),
+            dma((2 * pieces,)),
+            dma((2 * pieces,)),
+        ],
+        compiler_params=pltpu.CompilerParams(collective_id=0, has_side_effects=True),
+        name="exchange_weights",
+    )(packed)[0]
+
+
+def expert_kernel(rows_ref, weight_ref, joined_ref, gate_ref, up_ref, down_ref, sum_ref):
+    @pl.when(pl.program_id(0) == 0)
+    def _():
+        sum_ref[...] = jnp.zeros_like(sum_ref)
+
+    gate_ref[0] = joined_ref[0]
+    up_ref[0] = joined_ref[1]
+    down_ref[0] = joined_ref[2]
+    rows = rows_ref[...]
+    gate_act = jnp.dot(rows, joined_ref[0], preferred_element_type=jnp.float32)
+    up_act = jnp.dot(rows, joined_ref[1], preferred_element_type=jnp.float32)
+    hidden = (weight_ref[...] * jax.nn.silu(gate_act) * up_act).astype(jnp.bfloat16)
+    sum_ref[...] += lax.dot_general(
+        hidden, joined_ref[2], (((1,), (1,)), ((), ())), preferred_element_type=jnp.float32
+    )
+
+
+def expert_block(rows_all, weight, joined):
+    matrices, depth, width = joined.shape
+    tile = width // 8
+    count = rows_all.shape[0]
+    serve = jax.ShapeDtypeStruct((1, depth, width), jnp.bfloat16)
+    block = pl.BlockSpec((1, depth, tile), lambda i: (0, 0, i))
+    whole = lambda i: (0, 0)
+    return pl.pallas_call(
+        expert_kernel,
+        grid=(width // tile,),
+        in_specs=[
+            pl.BlockSpec((count, depth), whole),
+            pl.BlockSpec((count, 1), whole),
+            pl.BlockSpec((matrices, depth, tile), lambda i: (0, 0, i)),
+        ],
+        out_specs=[block, block, block, pl.BlockSpec((count, depth), whole)],
+        out_shape=[serve, serve, serve, jax.ShapeDtypeStruct((count, depth), jnp.float32)],
+        name="expert_block",
+    )(rows_all, weight, joined)
+
+
+def per_device(tokens, route_experts, route_logits, norm_gain, gate_train, up_train, down_train):
+    fs_size = lax.axis_size("fs")
+    expert_count = gate_train.shape[0]
+    slices = fs_size // expert_count
+    normed = normalize(tokens)
+    first = jax.nn.sigmoid(route_logits[:, 0] - route_logits[:, 1])
+    second = jax.nn.sigmoid(route_logits[:, 1] - route_logits[:, 0])
+    labels = jnp.arange(expert_count, dtype=jnp.int32)
+    table = first[:, None] * (route_experts[:, 0:1] == labels[None, :]).astype(jnp.float32)
+    table = table + second[:, None] * (route_experts[:, 1:2] == labels[None, :]).astype(jnp.float32)
+    table = table.astype(jnp.bfloat16)
+    rows_all, table_all = (
+        lax.all_gather(normed, "fs", axis=0, tiled=True),
+        lax.all_gather(table, "fs", axis=0, tiled=True),
+    )
+    own_expert = lax.axis_index("fs") // slices
+    selector = (labels == own_expert).astype(jnp.float32)
+    weight = jnp.sum(table_all.astype(jnp.float32) * selector[None, :], axis=1)
+    joined = exchanged(rounded(norm_gain, gate_train, up_train, down_train), fs_size)
+    gate_serve, up_serve, down_serve, partial = expert_block(rows_all, weight[:, None], joined)
+    summed = lax.psum_scatter(partial, "fs", scatter_dimension=0, tiled=True)
+    return (gate_serve, up_serve, down_serve, summed.astype(jnp.bfloat16))
+
+
+def two_by_two(fs_size, tp_size, experts):
+    return fs_size == 2 * experts and tp_size == 4
+
+
+def choose(*args):
+    fits = two_by_two(lax.axis_size("fs"), lax.axis_size("tp"), args[4].shape[0])
+    return (per_device if fits else per_device_general)(*args)
+
+
 def solution(mesh):
     return jax.shard_map(
-        per_device,
+        choose,
         mesh=mesh,
         in_specs=(
             P(("fs", "tp"), None),

time: 841 us -> 520 us (0.62)
  blocking collectives: 624 us -> 113 us
  Pallas kernels: 0 us -> 397 us
  local copies, waits for them, and re-layouts: 117 us -> 4.99 us
  waiting for transfers between devices: 44.4 us -> 0 us
  matrix products: 21.9 us -> 0 us
  between operations: 14.8 us -> 1.35 us
  other arithmetic: 12.7 us -> 3.7 us
    all_to_all x6 -> x0, blocking collectives: 536 us -> none  [the longest x3 292 us: per_device(): lax.all_to_all(for_sending(tuple((split_quarter(matrix) for matrix in swa...]
    pallas_call x0 -> x3, Pallas kernels: none -> 397 us  [the longest x1 348 us: exchanged(): pl.pallas_call(exchange_kernel, in_specs=[anywhere], out_specs=[anywhere,...]
    all_gather x3 -> x0, waiting for transfers between devices: 44.4 us -> none  [per_device(): lax.all_gather(for_sending(stacked), 'tp', axis=2, tiled=True)]
    unnamed x24 -> x4, local copies, waits for them, and re-layouts: 43.5 us -> 1.25 us
    reshape x3 -> x0, local copies, waits for them, and re-layouts: 30.7 us -> none  [split_quarter(): blocks = matrix.reshape(expert_count, quarter, slices, block_width)]
    dot_general x2 -> x0, matrix products: 21.9 us -> none  [the longest x1 13.9 us: per_device(): lax.dot_general(hidden, down_own, (((1,), (1,)), ((), ())), preferred_ele...]
    unnamed x1, blocking collectives: 38.3 us -> 59.8 us
    all_to_all x3 -> x0, local copies, waits for them, and re-layouts: 15.8 us -> none  [the longest x1 5.25 us: per_device(): lax.all_to_all(gate_half, 'tp', split_axis=1, concat_axis=2, tiled=True)]
  transfers between devices with their start and end apart: 3 -> 0, of which waited for: 1 -> 0; matrix products, arithmetic and copies ran while one was open for 8% -> 0% of each run, Pallas kernels for 0% -> 0%
where the time goes in v1:
time: 520 us; the launch traced here: 519 us
  Pallas kernels  397 us (76%)
  blocking collectives  113 us (22%)
    pallas_call x1, Pallas kernels, exchanged(): pl.pallas_call(exchange_kernel, in_specs=[anywhere], out_specs=[anywhere,...  348 us
    unnamed x1, blocking collectives  59.8 us
    pallas_call x1, Pallas kernels, expert_block(): pl.pallas_call(expert_kernel, grid=(width // tile,), in_specs=[pl.BlockSp...  33.9 us
    all_gather x1, blocking collectives, per_device(): lax.all_gather(normed, 'fs', axis=0, tiled=True)  30.5 us
    all_gather x1, blocking collectives, per_device(): lax.all_gather(table, 'fs', axis=0, tiled=True)  22.3 us
    pallas_call x1, Pallas kernels, rounded(): pl.pallas_call(round_kernel, grid=(experts, rows // tile), in_specs=[pl.B...  14.4 us

profile of v1, /device:TPU:0, one launch (start us, length us, event | category | flops | bytes accessed | tf_op | source)
XLA Modules:
  0.0 519.2 jit_solution(14645332831376764778)
XLA Ops:
  0.7 1.0 slice_reduce_fusion.1
  1.6 1.0 fusion.8
  2.6 0.1 fusion.10
  2.7 22.3 %all-gather.1 = bf16[8,2,4]{2,1,0:T(2,128)(2,1)S(1)} all-gather(bf16[1,2,4]{2,1,0:T(2,128)(2,1)S(1)} %fusion.10), channel_id=1, replica_groups=mesh['fs'=8,'tp'=4] {'fs'}, dimensions={0}, use_global_device_ids=true | all-gather | bytes 144 | tf_op jit(solution)/shard_map/all_gather | solution.py:358
  24.9 0.1 fusion.4
  25.1 0.7 copy.15.weight_ref
  25.8 0.8 convert_reduce_fusion
  26.6 0.9 fusion.2
  27.5 0.8 fusion.5
  28.3 30.5 %all-gather = bf16[8,2,2048]{2,1,0:T(2,128)(2,1)S(1)} all-gather(bf16[1,2,2048]{2,1,0:T(2,128)(2,1)S(1)} %fusion.5), channel_id=1, replica_groups=mesh['fs'=8,'tp'=4] {'fs'}, dimensions={0}, use_global_device_ids=true | all-gather | bytes 73728 | tf_op jit(solution)/shard_map/all_gather | solution.py:357
  58.8 0.7 reshape.26.rows_ref
  59.5 1.5 copy.14.gain_ref
  60.9 14.4 %round_weights.1.src = bf16[3,4,256,2048]{3,2,1,0:T(8,128)(2,1)} custom-call(f32[256,1]{1,0:T(8,128)} %copy.14.gain_ref, f32[4,256,2048]{2,1,0:T(8,128)} %gate_ref.1, f32[4,256,2048]{2,1,0:T(8,128)} %up_ref.1, f32[4,256,2048]{2,1,0:T(8,128)} %down_ref.1), custom_call_target="tpu_custom_call" | custom-call | tf_op jit(solution)/shard_map/round_weights/pallas_call | solution.py:106
  75.4 348.3 %exchange_weights.1 = (bf16[3,2048,4096]{2,1,0:T(8,128)(2,1)}, bf16[3,4,256,2048]{3,2,1,0:T(8,128)(2,1)}) custom-call(bf16[3,4,256,2048]{3,2,1,0:T(8,128)(2,1)} %round_weights.1.src), custom_call_target="tpu_custom_call" | custom-call | tf_op jit(solution)/shard_map/exchange_weights/pallas_call | solution.py:281
  423.7 0.0 copy-start
  423.7 33.9 %expert_block.1 = (bf16[1,2048,4096]{2,1,0:T(8,128)(2,1)}, bf16[1,2048,4096]{2,1,0:T(8,128)(2,1)}, bf16[1,2048,4096]{2,1,0:T(8,128)(2,1)}, f32[16,2048]{1,0:T(8,128)}) custom-call(bf16[16,2048]{1,0:T(8,128)(2,1)} %reshape.26.rows_ref, f32[16,1]{1,0:T(8,128)} %copy.15.weight_ref, bf16[3,2048,4096]{2,1,0:T(8,128)(2,1)} %get-tuple-element.9.joined_ref), custom_call_target="tpu_custom_call" | custom-call | tf_op jit(solution)/shard_map/expert_block/pallas_call | solution.py:331
  457.6 59.8 %all-reduce.2 = bf16[16,2048]{1,0:T(8,128)(2,1)S(1)} all-reduce(f32[16,2048]{1,0:T(8,128)} %get-tuple-element.13), channel_id=2, replica_groups=mesh['fs'=8,'tp'=4] {'fs'}, use_global_device_ids=true, to_apply=%region_3.4.clone | all-reduce | flops 32768 | bytes 196608
  517.4 0.0 copy-done
  517.4 0.6 dynamic-slice
  518.6 0.6 dynamic-slice_convert_fusion
  (3 shorter events, 0.0 us)
Async XLA Ops:
  423.7 93.7 %copy-start = (u32[32]{0:T(128)S(1)}, u32[32]{0:T(128)}, u32[]{:S(2)}) copy-start(u32[32]{0:T(128)} %constant.37) | copy-start | bytes 388

commit v2 on v1

--- a/solution.py
+++ b/solution.py
@@ -8,9 +8,10 @@
 from jax.sharding import PartitionSpec as P
 
 MESH = pl.DeviceIdType.MESH
-PARTS = 2
-LAG_TP = 2
-LAG_FS = 4
+PARTS = 4
+LAG_TP = 3
+LAG_FS = 6
+PAD = 128
 
 
 def for_sending(array):
@@ -114,7 +115,8 @@
 
 
 def exchange_kernel(
-    src, joined, transit, held, l_in, l_out, z_s, z_r, y_s, y_r, x_s, x_r, c_s, c_r
+    src, mine_ref, joined, transit, all_ref, held, l_in, l_out, z_s, z_r, y_s, y_r, x_s, x_r,
+    c_s, c_r, g_s, g_r
 ):
     matrices, experts, rows, width = src.shape
     chunk = rows // PARTS
@@ -131,9 +133,9 @@
         return (lax.rem(z + d, experts) * 2 + x, t)
 
     barrier = pltpu.get_barrier_semaphore()
-    for d in range(1, experts):
-        pl.semaphore_signal(barrier, inc=1, device_id=z_peer(d), device_id_type=MESH)
-    for peer in (y_peer, c_peer, x_peer):
+    fs_size = all_ref.shape[0]
+    fs_peers = [(lax.rem(f + q, fs_size), t) for q in range(1, fs_size)]
+    for peer in (*fs_peers, y_peer, c_peer):
         pl.semaphore_signal(barrier, inc=1, device_id=peer, device_id_type=MESH)
 
     def parts_of(k):
@@ -166,7 +168,10 @@
     def _(g):
         load(g).start()
 
-    pl.semaphore_wait(barrier, experts + 2)
+    all_ref[f] = mine_ref[...]
+    pl.semaphore_wait(barrier, fs_size + 1)
+    for q, peer in enumerate(fs_peers):
+        remote(mine_ref, all_ref.at[f], g_s.at[q], g_r.at[q], peer).start()
 
     def send_z(home):
         @pl.loop(0, pieces)
@@ -271,20 +276,26 @@
     def _():
         run(False)
 
-
-def exchanged(packed, fs_size):
+    for q, peer in enumerate(fs_peers):
+        owner = lax.rem(f + fs_size - q - 1, fs_size)
+        remote(mine_ref, all_ref.at[owner], g_s.at[q], g_r.at[q], peer).wait()
+
+
+def exchanged(packed, mine, fs_size):
     matrices, experts, rows, width = packed.shape
     pieces = matrices * PARTS * experts
     groups = matrices * PARTS
     anywhere = pl.BlockSpec(memory_space=pl.ANY)
+    in_vmem = pl.BlockSpec(memory_space=pltpu.VMEM)
     dma = pltpu.SemaphoreType.DMA
     return pl.pallas_call(
         exchange_kernel,
-        in_specs=[anywhere],
-        out_specs=[anywhere, anywhere],
+        in_specs=[anywhere, in_vmem],
+        out_specs=[anywhere, anywhere, in_vmem],
         out_shape=[
             jax.ShapeDtypeStruct((matrices, fs_size * rows, 2 * width), jnp.bfloat16),
             jax.ShapeDtypeStruct(packed.shape, jnp.bfloat16),
+            jax.ShapeDtypeStruct((fs_size, *mine.shape), jnp.bfloat16),
         ],
         scratch_shapes=[
             pltpu.VMEM((groups, rows // PARTS, width), jnp.bfloat16),
@@ -298,10 +309,12 @@
             dma((pieces,)),
             dma((2 * pieces,)),
             dma((2 * pieces,)),
+            dma((fs_size - 1,)),
+            dma((fs_size - 1,)),
         ],
         compiler_params=pltpu.CompilerParams(collective_id=0, has_side_effects=True),
         name="exchange_weights",
-    )(packed)[0]
+    )(packed, mine)
 
 
 def expert_kernel(rows_ref, weight_ref, joined_ref, gate_ref, up_ref, down_ref, sum_ref):
@@ -342,6 +355,49 @@
     )(rows_all, weight, joined)
 
 
+def reduce_kernel(part_ref, out_ref, landed, send, recv):
+    f = lax.axis_index("fs")
+    t = lax.axis_index("tp")
+    fs_size = part_ref.shape[0]
+    peers = [lax.rem(f + q, fs_size) for q in range(1, fs_size)]
+    barrier = pltpu.get_barrier_semaphore()
+    for peer in peers:
+        pl.semaphore_signal(barrier, inc=1, device_id=(peer, t), device_id_type=MESH)
+    pl.semaphore_wait(barrier, fs_size - 1)
+
+    def copy(q, slot):
+        return pltpu.make_async_remote_copy(
+            src_ref=part_ref.at[peers[q]], dst_ref=landed.at[slot], send_sem=send.at[q],
+            recv_sem=recv.at[q], device_id=(peers[q], t), device_id_type=MESH,
+        )
+
+    for q in range(fs_size - 1):
+        copy(q, q).start()
+    total = part_ref[f]
+    for q in range(fs_size - 1):
+        copy(q, q).wait()
+        total = total + landed[q]
+    out_ref[...] = total.astype(out_ref.dtype)
+
+
+def reduced(part):
+    fs_size, count, depth = part.shape
+    in_vmem = pl.BlockSpec(memory_space=pltpu.VMEM)
+    return pl.pallas_call(
+        reduce_kernel,
+        in_specs=[in_vmem],
+        out_specs=in_vmem,
+        out_shape=jax.ShapeDtypeStruct((count, depth), jnp.bfloat16),
+        scratch_shapes=[
+            pltpu.VMEM((fs_size - 1, count, depth), jnp.float32),
+            pltpu.SemaphoreType.DMA((fs_size - 1,)),
+            pltpu.SemaphoreType.DMA((fs_size - 1,)),
+        ],
+        compiler_params=pltpu.CompilerParams(collective_id=1, has_side_effects=True),
+        name="reduce_rows",
+    )(part)
+
+
 def per_device(tokens, route_experts, route_logits, norm_gain, gate_train, up_train, down_train):
     fs_size = lax.axis_size("fs")
     expert_count = gate_train.shape[0]
@@ -349,25 +405,26 @@
     normed = normalize(tokens)
     first = jax.nn.sigmoid(route_logits[:, 0] - route_logits[:, 1])
     second = jax.nn.sigmoid(route_logits[:, 1] - route_logits[:, 0])
-    labels = jnp.arange(expert_count, dtype=jnp.int32)
+    labels = jnp.arange(PAD, dtype=jnp.int32)
     table = first[:, None] * (route_experts[:, 0:1] == labels[None, :]).astype(jnp.float32)
     table = table + second[:, None] * (route_experts[:, 1:2] == labels[None, :]).astype(jnp.float32)
     table = table.astype(jnp.bfloat16)
-    rows_all, table_all = (
-        lax.all_gather(normed, "fs", axis=0, tiled=True),
-        lax.all_gather(table, "fs", axis=0, tiled=True),
-    )
+    packed = rounded(norm_gain, gate_train, up_train, down_train)
+    mine = jnp.concatenate([normed, table], axis=1)
+    joined, _, gathered = exchanged(packed, mine, fs_size)
+    count, depth = tokens.shape
+    gathered = gathered.reshape(fs_size * count, depth + PAD)
+    rows_all, table_all = gathered[:, :depth], gathered[:, depth:]
     own_expert = lax.axis_index("fs") // slices
     selector = (labels == own_expert).astype(jnp.float32)
     weight = jnp.sum(table_all.astype(jnp.float32) * selector[None, :], axis=1)
-    joined = exchanged(rounded(norm_gain, gate_train, up_train, down_train), fs_size)
     gate_serve, up_serve, down_serve, partial = expert_block(rows_all, weight[:, None], joined)
-    summed = lax.psum_scatter(partial, "fs", scatter_dimension=0, tiled=True)
-    return (gate_serve, up_serve, down_serve, summed.astype(jnp.bfloat16))
+    mixed = reduced(partial.reshape(fs_size, count, depth))
+    return (gate_serve, up_serve, down_serve, mixed)
 
 
 def two_by_two(fs_size, tp_size, experts):
-    return fs_size == 2 * experts and tp_size == 4
+    return fs_size == 2 * experts and tp_size == 4 and experts <= PAD
 
 
 def choose(*args):

time: 520 us -> 446 us (0.86)
  blocking collectives: 113 us -> 0 us
  Pallas kernels: 397 us -> 433 us
    unnamed x1 -> x0, blocking collectives: 59.8 us -> none
    all_gather x2 -> x0, blocking collectives: 52.8 us -> none  [the longest x1 30.5 us: per_device(): lax.all_gather(normed, 'fs', axis=0, tiled=True)]
    pallas_call x1 -> x2, Pallas kernels: 348 us -> 385 us  [the longest x1 365 us: exchanged(): pl.pallas_call(exchange_kernel, in_specs=[anywhere, in_vmem], out_specs=[...]
where the time goes in v2:
time: 446 us
  Pallas kernels  433 us (97%)
  local copies, waits for them, and re-layouts  7.58 us (2%)
    pallas_call x1, Pallas kernels, exchanged(): pl.pallas_call(exchange_kernel, in_specs=[anywhere, in_vmem], out_specs=[...  365 us
    pallas_call x1, Pallas kernels, expert_block(): pl.pallas_call(expert_kernel, grid=(width // tile,), in_specs=[pl.BlockSp...  33.9 us
    pallas_call x1, Pallas kernels, reduced(): pl.pallas_call(reduce_kernel, in_specs=[in_vmem], out_specs=in_vmem, out_...  20.2 us
    pallas_call x1, Pallas kernels, rounded(): pl.pallas_call(round_kernel, grid=(experts, rows // tile), in_specs=[pl.B...  14.4 us

profile of v2, /device:TPU:0, one launch (start us, length us, event | category | flops | bytes accessed | tf_op | source)
XLA Modules:
  0.0 445.7 jit_solution(15787218041403696959)
XLA Ops:
  0.7 0.8 convert_reduce_fusion
  1.5 0.9 fusion.2
  2.4 1.0 slice_reduce_fusion.1
  3.4 1.0 fusion.6
  4.4 0.1 fusion.5
  4.4 0.8 fusion.3
  5.2 0.6 pad_maximum_fusion.mine_ref
  5.8 1.5 copy.12.gain_ref
  7.3 14.4 %round_weights.1.src = bf16[3,4,256,2048]{3,2,1,0:T(8,128)(2,1)} custom-call(f32[256,1]{1,0:T(8,128)} %copy.12.gain_ref, f32[4,256,2048]{2,1,0:T(8,128)} %gate_ref.1, f32[4,256,2048]{2,1,0:T(8,128)} %up_ref.1, f32[4,256,2048]{2,1,0:T(8,128)} %down_ref.1), custom_call_target="tpu_custom_call" | custom-call | tf_op jit(solution)/shard_map/round_weights/pallas_call | solution.py:107
  21.7 364.6 %exchange_weights.1 = (bf16[3,2048,4096]{2,1,0:T(8,128)(2,1)}, bf16[3,4,256,2048]{3,2,1,0:T(8,128)(2,1)}, bf16[8,2,2176]{2,1,0:T(2,128)(2,1)}) custom-call(bf16[3,4,256,2048]{3,2,1,0:T(8,128)(2,1)} %round_weights.1.src, bf16[2,2176]{1,0:T(2,128)(2,1)} %pad_maximum_fusion.mine_ref), custom_call_target="tpu_custom_call" | custom-call | tf_op jit(solution)/shard_map/exchange_weights/pallas_call | solution.py:291
  386.3 0.9 reshape.31
  387.3 0.1 multiply_reduce_fusion
  387.4 0.6 slice.26.rows_ref
  388.0 0.7 copy.13.weight_ref
  388.7 33.9 %expert_block.1 = (bf16[1,2048,4096]{2,1,0:T(8,128)(2,1)}, bf16[1,2048,4096]{2,1,0:T(8,128)(2,1)}, bf16[1,2048,4096]{2,1,0:T(8,128)(2,1)}, f32[16,2048]{1,0:T(8,128)}) custom-call(bf16[16,2048]{1,0:T(8,128)(2,1)} %slice.26.rows_ref, f32[16,1]{1,0:T(8,128)} %copy.13.weight_ref, bf16[3,2048,4096]{2,1,0:T(8,128)(2,1)} %get-tuple-element.11.joined_ref), custom_call_target="tpu_custom_call" | custom-call | tf_op jit(solution)/shard_map/expert_block/pallas_call | solution.py:344
  422.6 1.6 reshape.32.part_ref
  424.2 20.2 %reduce_rows.1 = bf16[2,2048]{1,0:T(2,128)(2,1)} custom-call(f32[8,2,2048]{2,1,0:T(2,128)} %reshape.32.part_ref), custom_call_target="tpu_custom_call" | custom-call | tf_op jit(solution)/shard_map/reduce_rows/pallas_call | solution.py:386
  444.4 1.3 copy.15
  (3 shorter events, 0.0 us)
